TPU v7x, 128 devices: a whole 4x4x4 slice. The times are simulated.
128 devices in a mesh: fs: 16 (over z, x), tp: 8 (over y, core).
Axes of the slice: x: 4, y: 4, z: 4, core: 2. Of those that a mesh axis runs over, the one named last changes fastest.
Arguments:
- tokens: bfloat16 [32, 384, 2048], P('fs', None, 'tp'), may hold values from -20 to 20
- first_gain: float32 [2048], replicated, may hold values from 0.1 to 1.9
- first_gate: bfloat16 [2048, 5120], P('fs', 'tp'), may hold values from -0.125 to 0.125
- first_up: bfloat16 [2048, 5120], P('fs', 'tp'), may hold values from -0.125 to 0.125
- first_down: bfloat16 [5120, 2048], P('tp', 'fs'), may hold values from -0.078125 to 0.078125
- mixer_gain: float32 [2048], replicated, may hold values from 0.1 to 1.9
- conv_input: bfloat16 [2048, 1024], P('fs', 'tp'), may hold values from -0.125 to 0.125
- outer_gate: bfloat16 [2048, 1024], P('fs', 'tp'), may hold values from -0.125 to 0.125
- inner_gate: bfloat16 [2048, 1024], P('fs', 'tp'), may hold values from -0.125 to 0.125
- conv_taps: float32 [3, 1024], P(None, 'tp'), may hold values from -3.5 to 3.5
- mixer_out: bfloat16 [1024, 2048], P('tp', 'fs'), may hold values from -0.1875 to 0.1875
- second_gain: float32 [2048], replicated, may hold values from 0.1 to 1.9
- second_gate: bfloat16 [2048, 5120], P('fs', 'tp'), may hold values from -0.125 to 0.125
- second_up: bfloat16 [2048, 5120], P('fs', 'tp'), may hold values from -0.125 to 0.125
- second_down: bfloat16 [5120, 2048], P('tp', 'fs'), may hold values from -0.078125 to 0.078125
Outputs:
- layer_out: bfloat16 [32, 384, 2048], P('fs', None, 'tp')
All inputs are finite; a program needn't handle non-finite values.
Results may differ from a plain program's by a relative error of at most 0.015.
Values may be sent and summed in bfloat16 or wider, within the bound.
A program may use at most 64 MiB of HBM per device.

v0:
```python
import jax
import jax.numpy as jnp
from jax import lax
from jax.sharding import PartitionSpec as P

epsilon = 1e-05


def sent_together(arrays, axis, dim, along):
    ends, at = ([], 0)
    for a in arrays[:-1]:
        at += a.shape[along]
        ends.append(at)
    both = jnp.concatenate(arrays, axis=along)
    return tuple(jnp.split(lax.all_gather(both, axis, axis=dim, tiled=True), ends, axis=along))


def copy_for_each(value, axis):
    copies = jnp.broadcast_to(value, (lax.axis_size(axis), *value.shape))
    return lax.all_to_all(copies, axis, split_axis=0, concat_axis=0, tiled=True)


def joined_along(pieces, dim):
    shape = list(pieces.shape[1:])
    shape[dim] *= pieces.shape[0]
    return jnp.moveaxis(pieces, 0, dim).reshape(shape)


def gathered_copies(value, axis, dim):
    pieces = copy_for_each(value, axis)
    return joined_along(pieces, dim)


def norm_rows(stream, gain):
    whole = lax.all_gather(stream, "tp", axis=1, tiled=True)
    values = whole.astype(jnp.float32)
    scale = lax.rsqrt(jnp.mean(values * values, axis=1, keepdims=True) + epsilon)
    return (values * scale * gain).astype(jnp.bfloat16)


def add_rows(gathered, piece):
    return jnp.dot(gathered, piece, preferred_element_type=jnp.float32)


def ffn_inputs(gathered, gate_weight, up_weight):
    pieces = sent_together((gate_weight, up_weight), "fs", 0, 1)
    gate = add_rows(gathered, pieces[0])
    upward = add_rows(gathered, pieces[1])
    return (gate, upward)


def mixer_inputs(gathered, conv_input, outer_gate, inner_gate):
    pieces = sent_together((conv_input, outer_gate, inner_gate), "fs", 0, 1)
    conv_values = add_rows(gathered, pieces[0])
    outer = add_rows(gathered, pieces[1])
    inner = add_rows(gathered, pieces[2])
    return (conv_values, outer, inner)


def project_down(hidden, weight):
    partial_sum = jnp.dot(
        hidden, gathered_copies(weight, "fs", 1), preferred_element_type=jnp.float32
    )
    result = lax.psum_scatter(
        partial_sum.astype(jnp.bfloat16), "tp", scatter_dimension=1, tiled=True
    ).astype(jnp.float32)
    return result


def half_ffn(stream, gain, gate_weight, up_weight, down_weight):
    gathered = norm_rows(stream, gain)
    gate, upward = ffn_inputs(gathered, gate_weight, up_weight)
    hidden = (jax.nn.silu(gate) * upward).astype(jnp.bfloat16)
    branch = project_down(hidden, down_weight)
    return (stream.astype(jnp.float32) + 0.5 * branch).astype(jnp.bfloat16)


def conv_mixer(stream, seqs, gain, conv_input, outer_gate, inner_gate, conv_taps, mixer_out):
    gathered = norm_rows(stream, gain)
    conv_values, outer, inner = mixer_inputs(gathered, conv_input, outer_gate, inner_gate)
    gated_input = (inner * conv_values).reshape(seqs, -1, conv_values.shape[1])
    one_back = jnp.pad(gated_input, ((0, 0), (1, 0), (0, 0)))[:, :-1]
    two_back = jnp.pad(gated_input, ((0, 0), (2, 0), (0, 0)))[:, :-2]
    convolved = conv_taps[0] * two_back + conv_taps[1] * one_back + conv_taps[2] * gated_input
    mixed = (outer * convolved.reshape(conv_values.shape)).astype(jnp.bfloat16)
    branch = project_down(mixed, mixer_out)
    return (stream.astype(jnp.float32) + branch).astype(jnp.bfloat16)


def on_device(
    tokens,
    first_gain,
    first_gate,
    first_up,
    first_down,
    mixer_gain,
    conv_input,
    outer_gate,
    inner_gate,
    conv_taps,
    mixer_out,
    second_gain,
    second_gate,
    second_up,
    second_down,
):
    seqs, length, width = tokens.shape
    stream = tokens.reshape(seqs * length, width)
    stream = half_ffn(stream, first_gain, first_gate, first_up, first_down)
    stream = conv_mixer(
        stream, seqs, mixer_gain, conv_input, outer_gate, inner_gate, conv_taps, mixer_out
    )
    stream = half_ffn(stream, second_gain, second_gate, second_up, second_down)
    return stream.reshape(seqs, length, width)


def solution(mesh):
    in_specs = (
        P("fs", None, "tp"),
        P(),
        P("fs", "tp"),
        P("fs", "tp"),
        P("tp", "fs"),
        P(),
        P("fs", "tp"),
        P("fs", "tp"),
        P("fs", "tp"),
        P(None, "tp"),
        P("tp", "fs"),
        P(),
        P("fs", "tp"),
        P("fs", "tp"),
        P("tp", "fs"),
    )
    out_specs = P("fs", None, "tp")
    return jax.shard_map(
        on_device, mesh=mesh, in_specs=in_specs, out_specs=out_specs, check_vma=False
    )
```

profile of v0, /device:TPU:0, one launch (start us, length us, event | category | flops | bytes accessed | tf_op | source)
XLA Modules:
  0.0 431.1 jit_solution(13457404551450091952)
XLA Ops:
  6.5 0.0 all-gather.7.cloned.1.call-start
  6.5 0.7 all-gather.7.cloned.1.call-update
  7.3 0.0 all-gather.9.cloned.1.call-start
  7.3 1.7 pad_maximum_fusion
  9.0 0.0 all-gather.9.cloned.1.call-update
  9.1 1.1 copy.16
  10.1 1.9 broadcast_in_dim.6
  12.0 8.2 %all-to-all-start = ((bf16[16,640,128]{1,2,0:T(8,128)(2,1)}), bf16[16,640,128]{1,2,0:T(8,128)(2,1)}, u32[]{:S(2)}, u32[]{:S(2)}) async-start(bf16[16,640,128]{1,2,0:T(8,128)(2,1)} %broadcast_in_dim.6), calls=%async_computation | async-start | bytes 5242880 | tf_op jit(solution)/shard_map/all_to_all | solution.py:20
  20.2 0.0 reduce-scatter.4.cloned.1.call-start
  20.3 22.4 %all-gather.7.cloned.1.call-done = bf16[768,2048]{1,0:T(8,128)(2,1)} async-done(((bf16[768,256]{1,0:T(8,128)(2,1)}), bf16[768,2048]{1,0:T(8,128)(2,1)}) %all-gather.7.cloned.1.call-update) | async-done | bytes 3145744 | tf_op jit(solution)/shard_map/all_gather | solution.py:35
  42.7 2.7 fusion
  45.4 56.7 %all-gather.9.cloned.1.call-done = bf16[2048,1280]{1,0:T(8,128)(2,1)} async-done(((bf16[128,1280]{1,0:T(8,128)(2,1)}), bf16[2048,1280]{1,0:T(8,128)(2,1)}) %all-gather.9.cloned.1.call-update) | async-done | bytes 5242896 | tf_op jit(solution)/shard_map/all_gather | solution.py:15
  102.1 0.0 copy-done.15
  102.1 0.0 copy-done.3
  102.1 5.7 %fusion.15 = f32[768,640]{1,0:T(8,128)} fusion(bf16[2048,1280]{1,0:T(8,128)(2,1)} %all-gather.9.cloned.1.call-done, bf16[768,2048]{1,0:T(8,128)(2,1)S(1)} %copy-done.3, f32[2048]{0:T(1024)S(1)} %copy-done.15, f32[768]{0:T(1024)S(1)} %add_rsqrt_fusion.2), kind=kOutput, calls=%fused_computation.24 | convolution fusion | flops 2019557376 | bytes 7744512 | tf_op jit(solution)/shard_map/dot_general | solution.py:42
  107.8 0.0 all-to-all-done
  107.8 10.7 %convolution_convert_fusion.1 = bf16[768,2048]{1,0:T(8,128)(2,1)} fusion(bf16[640,2048]{0,1:T(8,128)(2,1)} %bitcast.2, f32[768,640]{1,0:T(8,128)} %fusion.15, bf16[2048,1280]{1,0:T(8,128)(2,1)} %all-gather.9.cloned.1.call-done, bf16[768,2048]{1,0:T(8,128)(2,1)S(1)} %copy-done.3, f32[2048]{0:T(1024)S(1)} %copy-done.15, f32[768]{0:T(1024)S(1)} %add_rsqrt_fusion.2), kind=kOutput, calls=%fused_computation.16 | convolution fusion | flops 4037345280 | bytes 13511680 | tf_op jit(solution)/shard_map/dot_general | solution.py:61
  118.5 0.0 copy-start.9
  118.5 0.0 copy-start.14
  118.5 0.0 reduce-scatter.4.cloned.1.call-update
  118.5 0.0 copy-start.13
  118.6 0.0 all-gather.11.cloned.1.call-start
  118.6 35.6 %reduce-scatter.4.cloned.1.call-done = bf16[768,256]{1,0:T(8,128)(2,1)} async-done(((bf16[768,2048]{1,0:T(8,128)(2,1)}), bf16[768,256]{1,0:T(8,128)(2,1)}) %reduce-scatter.4.cloned.1.call-update) | async-done | bytes 393232 | tf_op jit(solution)/shard_map/reduce_scatter | solution.py:64
  154.2 1.9 add_convert_fusion.2
  156.1 0.0 all-gather.11.cloned.1.call-update
  156.1 0.0 all-gather.13.cloned.1.call-start
  156.2 0.6 pad_maximum_fusion.2
  156.8 0.0 all-gather.13.cloned.1.call-update
  156.8 0.0 copy-done.9
  156.9 0.1 copy.17
  157.0 0.9 broadcast_in_dim.7
  157.9 7.0 %all-to-all-start.1 = ((bf16[16,128,128]{1,2,0:T(8,128)(2,1)}), bf16[16,128,128]{1,2,0:T(8,128)(2,1)}, u32[]{:S(2)}, u32[]{:S(2)}) async-start(bf16[16,128,128]{1,2,0:T(8,128)(2,1)} %broadcast_in_dim.7), calls=%async_computation.2 | async-start | bytes 1048576 | tf_op jit(solution)/shard_map/all_to_all | solution.py:20
  164.9 0.2 reduce-scatter.6.cloned.1.call-start
  165.2 21.0 %all-gather.11.cloned.1.call-done = bf16[768,2048]{1,0:T(8,128)(2,1)} async-done(((bf16[768,256]{1,0:T(8,128)(2,1)}), bf16[768,2048]{1,0:T(8,128)(2,1)}) %all-gather.11.cloned.1.call-update) | async-done | bytes 3145744 | tf_op jit(solution)/shard_map/all_gather | solution.py:35
  186.2 2.7 fusion.3
  189.0 0.1 copy-done
  189.0 0.8 fusion.5
  189.8 43.1 %all-gather.13.cloned.1.call-done = bf16[2048,384]{1,0:T(8,128)(2,1)} async-done(((bf16[128,384]{1,0:T(8,128)(2,1)}), bf16[2048,384]{1,0:T(8,128)(2,1)}) %all-gather.13.cloned.1.call-update) | async-done | bytes 1572880 | tf_op jit(solution)/shard_map/all_gather | solution.py:15
  233.0 2.0 fusion.35
  235.0 2.0 convolution_multiply_fusion
  237.0 0.1 fusion.41
  237.1 0.0 all-to-all-done.1
  237.1 6.2 %convolution_convert_fusion.2 = bf16[768,2048]{1,0:T(8,128)(2,1)} fusion(bf16[128,2048]{0,1:T(8,128)(2,1)} %bitcast.9, f32[768,128]{1,0:T(8,128)S(1)} %bitcast.28, bf16[768,2048]{1,0:T(8,128)(2,1)S(1)} %fusion.5, bf16[2048,384]{1,0:T(8,128)(2,1)} %all-gather.13.cloned.1.call-done), kind=kOutput, calls=%fused_computation.17 | convolution fusion | flops 807075840 | bytes 7733248 | tf_op jit(solution)/shard_map/dot_general | solution.py:61
  243.3 0.0 reduce-scatter.6.cloned.1.call-update
  243.3 0.0 all-gather.15.cloned.1.call-start
  243.4 35.3 %reduce-scatter.6.cloned.1.call-done = bf16[768,256]{1,0:T(8,128)(2,1)} async-done(((bf16[768,2048]{1,0:T(8,128)(2,1)}), bf16[768,256]{1,0:T(8,128)(2,1)}) %reduce-scatter.6.cloned.1.call-update) | async-done | bytes 393232 | tf_op jit(solution)/shard_map/reduce_scatter | solution.py:64
  278.7 1.8 add_convert_fusion.1
  280.5 0.0 all-gather.15.cloned.1.call-update
  280.6 0.0 all-gather.17.cloned.1.call-start
  280.6 0.7 pad_maximum_fusion.1
  281.4 0.0 all-gather.17.cloned.1.call-update
  281.4 0.2 copy.18
  281.6 1.9 broadcast_in_dim.8
  283.5 7.1 %all-to-all-start.2 = ((bf16[16,640,128]{1,2,0:T(8,128)(2,1)}), bf16[16,640,128]{1,2,0:T(8,128)(2,1)}, u32[]{:S(2)}, u32[]{:S(2)}) async-start(bf16[16,640,128]{1,2,0:T(8,128)(2,1)} %broadcast_in_dim.8), calls=%async_computation.4 | async-start | bytes 5242880 | tf_op jit(solution)/shard_map/all_to_all | solution.py:20
  290.6 0.3 reduce-scatter.8.cloned.1.call-start
  290.9 19.8 %all-gather.15.cloned.1.call-done = bf16[768,2048]{1,0:T(8,128)(2,1)} async-done(((bf16[768,256]{1,0:T(8,128)(2,1)}), bf16[768,2048]{1,0:T(8,128)(2,1)}) %all-gather.15.cloned.1.call-update) | async-done | bytes 3145744 | tf_op jit(solution)/shard_map/all_gather | solution.py:35
  310.7 2.7 fusion.6
  313.4 57.2 %all-gather.17.cloned.1.call-done = bf16[2048,1280]{1,0:T(8,128)(2,1)} async-done(((bf16[128,1280]{1,0:T(8,128)(2,1)}), bf16[2048,1280]{1,0:T(8,128)(2,1)}) %all-gather.17.cloned.1.call-update) | async-done | bytes 5242896 | tf_op jit(solution)/shard_map/all_gather | solution.py:15
  370.6 5.7 %fusion.11 = f32[768,640]{1,0:T(8,128)} fusion(bf16[2048,1280]{1,0:T(8,128)(2,1)} %all-gather.17.cloned.1.call-done, bf16[768,2048]{1,0:T(8,128)(2,1)S(1)} %copy-done.4, f32[2048]{0:T(1024)S(1)} %copy-done.16, f32[768]{0:T(1024)S(1)} %add_rsqrt_fusion), kind=kOutput, calls=%fused_computation.20 | convolution fusion | flops 2019557376 | bytes 7744512 | tf_op jit(solution)/shard_map/dot_general | solution.py:42
  376.3 0.0 all-to-all-done.2
  376.3 10.7 %convolution_convert_fusion = bf16[768,2048]{1,0:T(8,128)(2,1)} fusion(bf16[640,2048]{0,1:T(8,128)(2,1)} %bitcast.11, f32[768,640]{1,0:T(8,128)} %fusion.11, bf16[2048,1280]{1,0:T(8,128)(2,1)} %all-gather.17.cloned.1.call-done, bf16[768,2048]{1,0:T(8,128)(2,1)S(1)} %copy-done.4, f32[2048]{0:T(1024)S(1)} %copy-done.16, f32[768]{0:T(1024)S(1)} %add_rsqrt_fusion), kind=kOutput, calls=%fused_computation.15 | convolution fusion | flops 4037345280 | bytes 13511680 | tf_op jit(solution)/shard_map/dot_general | solution.py:61
  387.0 0.0 reduce-scatter.8.cloned.1.call-update
  387.0 35.7 %reduce-scatter.8.cloned.1.call-done = bf16[768,256]{1,0:T(8,128)(2,1)} async-done(((bf16[768,2048]{1,0:T(8,128)(2,1)}), bf16[768,256]{1,0:T(8,128)(2,1)}) %reduce-scatter.8.cloned.1.call-update) | async-done | bytes 393232 | tf_op jit(solution)/shard_map/reduce_scatter | solution.py:64
  422.7 1.9 add_convert_fusion
  (31 shorter events, 0.1 us)
Async XLA Ops:
  6.5 36.1 %all-gather.7.cloned.1.call-start = ((), (), s32[]{:S(2)}) async-start(), calls=%async_computation.6 | async-start | bytes 3538944 | tf_op jit(solution)/shard_map/all_gather | solution.py:35
  7.3 94.8 %all-gather.9.cloned.1.call-start = ((), (), s32[]{:S(2)}) async-start(), calls=%async_computation.7 | async-start | bytes 5570560 | tf_op jit(solution)/shard_map/all_gather | solution.py:15
  12.0 90.1 %copy-start.15 = (f32[2048]{0:T(1024)S(1)}, f32[2048]{0:T(1024)}, u32[]{:S(2)}) copy-start(f32[2048]{0:T(1024)} %param.16) | copy-start | bytes 24580
  12.0 95.8 %all-to-all-start = ((bf16[16,640,128]{1,2,0:T(8,128)(2,1)}), bf16[16,640,128]{1,2,0:T(8,128)(2,1)}, u32[]{:S(2)}, u32[]{:S(2)}) async-start(bf16[16,640,128]{1,2,0:T(8,128)(2,1)} %broadcast_in_dim.6), calls=%async_computation | async-start | bytes 5242880 | tf_op jit(solution)/shard_map/all_to_all | solution.py:20
  20.2 134.0 %reduce-scatter.4.cloned.1.call-start = ((), (), s32[]{:S(2)}) async-start(), calls=%async_computation.8 | async-start | bytes 3538944 | tf_op jit(solution)/shard_map/reduce_scatter | solution.py:64
  42.7 59.5 %copy-start.3 = (bf16[768,2048]{1,0:T(8,128)(2,1)S(1)}, bf16[768,2048]{1,0:T(8,128)(2,1)}, u32[]{:S(2)}) copy-start(bf16[768,2048]{1,0:T(8,128)(2,1)} %all-gather.7.cloned.1.call-done) | copy-start | bytes 9437188
  118.5 35.7 %copy-start.5 = (bf16[2,384,256]{2,1,0:T(8,128)(2,1)S(1)}, bf16[2,384,256]{2,1,0:T(8,128)(2,1)}, u32[]{:S(2)}) copy-start(bf16[2,384,256]{2,1,0:T(8,128)(2,1)} %param.15) | copy-start | bytes 1179652
  118.5 37.7 %copy-start.10 = (bf16[128,128]{1,0:T(8,128)(2,1)S(1)}, bf16[128,128]{1,0:T(8,128)(2,1)}, u32[]{:S(2)}) copy-start(bf16[128,128]{1,0:T(8,128)(2,1)} %param.23) | copy-start | bytes 98308
  118.5 37.7 %copy-start.11 = (bf16[128,128]{1,0:T(8,128)(2,1)S(1)}, bf16[128,128]{1,0:T(8,128)(2,1)}, u32[]{:S(2)}) copy-start(bf16[128,128]{1,0:T(8,128)(2,1)} %param.22) | copy-start | bytes 98308
  118.5 37.7 %copy-start.12 = (bf16[128,128]{1,0:T(8,128)(2,1)S(1)}, bf16[128,128]{1,0:T(8,128)(2,1)}, u32[]{:S(2)}) copy-start(bf16[128,128]{1,0:T(8,128)(2,1)} %param.21) | copy-start | bytes 98308
  118.5 38.3 %copy-start.9 = (bf16[128,128]{1,0:T(8,128)(2,1)S(1)}, bf16[128,128]{1,0:T(8,128)(2,1)}, u32[]{:S(2)}) copy-start(bf16[128,128]{1,0:T(8,128)(2,1)} %param.25) | copy-start | bytes 98308
  118.5 46.6 %copy-start.14 = (f32[3,128]{1,0:T(4,128)S(1)}, f32[3,128]{1,0:T(4,128)}, u32[]{:S(2)}) copy-start(f32[3,128]{1,0:T(4,128)} %param.24) | copy-start | bytes 4612
  118.5 70.4 %copy-start.13 = (f32[2048]{0:T(1024)S(1)}, f32[2048]{0:T(1024)}, u32[]{:S(2)}) copy-start(f32[2048]{0:T(1024)} %param.20) | copy-start | bytes 24580
  118.6 67.6 %all-gather.11.cloned.1.call-start = ((), (), s32[]{:S(2)}) async-start(), calls=%async_computation.9 | async-start | bytes 3538944 | tf_op jit(solution)/shard_map/all_gather | solution.py:35
  156.1 76.9 %all-gather.13.cloned.1.call-start = ((), (), s32[]{:S(2)}) async-start(), calls=%async_computation.10 | async-start | bytes 1671168 | tf_op jit(solution)/shard_map/all_gather | solution.py:15
  157.9 79.2 %all-to-all-start.1 = ((bf16[16,128,128]{1,2,0:T(8,128)(2,1)}), bf16[16,128,128]{1,2,0:T(8,128)(2,1)}, u32[]{:S(2)}, u32[]{:S(2)}) async-start(bf16[16,128,128]{1,2,0:T(8,128)(2,1)} %broadcast_in_dim.7), calls=%async_computation.2 | async-start | bytes 1048576 | tf_op jit(solution)/shard_map/all_to_all | solution.py:20
  164.9 113.8 %reduce-scatter.6.cloned.1.call-start = ((), (), s32[]{:S(2)}) async-start(), calls=%async_computation.11 | async-start | bytes 3538944 | tf_op jit(solution)/shard_map/reduce_scatter | solution.py:64
  186.2 2.8 copy-start
  243.3 35.4 %copy-start.1 = (bf16[768,256]{1,0:T(8,128)(2,1)S(1)}, bf16[768,256]{1,0:T(8,128)(2,1)}, u32[]{:S(2)}) copy-start(bf16[768,256]{1,0:T(8,128)(2,1)} %add_convert_fusion.2) | copy-start | bytes 1179652
  243.3 37.3 %copy-start.6 = (bf16[128,640]{1,0:T(8,128)(2,1)S(1)}, bf16[128,640]{1,0:T(8,128)(2,1)}, u32[]{:S(2)}) copy-start(bf16[128,640]{1,0:T(8,128)(2,1)} %param.28) | copy-start | bytes 491524
  243.3 37.3 %copy-start.7 = (bf16[128,640]{1,0:T(8,128)(2,1)S(1)}, bf16[128,640]{1,0:T(8,128)(2,1)}, u32[]{:S(2)}) copy-start(bf16[128,640]{1,0:T(8,128)(2,1)} %param.27) | copy-start | bytes 491524
  243.3 38.1 %copy-start.8 = (bf16[640,128]{1,0:T(8,128)(2,1)S(1)}, bf16[640,128]{1,0:T(8,128)(2,1)}, u32[]{:S(2)}) copy-start(bf16[640,128]{1,0:T(8,128)(2,1)} %param.29) | copy-start | bytes 491524
  243.3 67.3 %all-gather.15.cloned.1.call-start = ((), (), s32[]{:S(2)}) async-start(), calls=%async_computation.12 | async-start | bytes 3538944 | tf_op jit(solution)/shard_map/all_gather | solution.py:35
  280.6 90.0 %all-gather.17.cloned.1.call-start = ((), (), s32[]{:S(2)}) async-start(), calls=%async_computation.13 | async-start | bytes 5570560 | tf_op jit(solution)/shard_map/all_gather | solution.py:15
  283.5 87.1 %copy-start.16 = (f32[2048]{0:T(1024)S(1)}, f32[2048]{0:T(1024)}, u32[]{:S(2)}) copy-start(f32[2048]{0:T(1024)} %param.26) | copy-start | bytes 24580
  283.5 92.8 %all-to-all-start.2 = ((bf16[16,640,128]{1,2,0:T(8,128)(2,1)}), bf16[16,640,128]{1,2,0:T(8,128)(2,1)}, u32[]{:S(2)}, u32[]{:S(2)}) async-start(bf16[16,640,128]{1,2,0:T(8,128)(2,1)} %broadcast_in_dim.8), calls=%async_computation.4 | async-start | bytes 5242880 | tf_op jit(solution)/shard_map/all_to_all | solution.py:20
  290.6 132.1 %reduce-scatter.8.cloned.1.call-start = ((), (), s32[]{:S(2)}) async-start(), calls=%async_computation.14 | async-start | bytes 3538944 | tf_op jit(solution)/shard_map/reduce_scatter | solution.py:64
  310.7 60.0 %copy-start.4 = (bf16[768,2048]{1,0:T(8,128)(2,1)S(1)}, bf16[768,2048]{1,0:T(8,128)(2,1)}, u32[]{:S(2)}) copy-start(bf16[768,2048]{1,0:T(8,128)(2,1)} %all-gather.15.cloned.1.call-done) | copy-start | bytes 9437188
  387.0 35.7 %copy-start.2 = (bf16[768,256]{1,0:T(8,128)(2,1)S(1)}, bf16[768,256]{1,0:T(8,128)(2,1)}, u32[]{:S(2)}) copy-start(bf16[768,256]{1,0:T(8,128)(2,1)} %add_convert_fusion.1) | copy-start | bytes 1179652
Sparse Core Ops, SparseCore 0:
  9.0 33.5 all-gather.6
  44.8 57.2 all-gather.8
  118.7 35.4 reduce-scatter.3
  156.2 29.9 all-gather.10
  188.2 44.7 all-gather.12
  243.5 35.2 reduce-scatter.5
  280.7 29.9 all-gather.14
  312.8 57.7 all-gather.16
  387.1 35.4 reduce-scatter.7
where the time goes:
time: 432 us; the launch traced here: 431 us
  waiting for transfers between devices  328 us (76%)
  matrix products  42.9 us (10%)
  starting transfers between devices  23 us (5%)
  other arithmetic  17.8 us (4%)
  between operations  13.4 us (3%)
  local copies, waits for them, and re-layouts  6.23 us (1%)
    all_gather x3, waiting for transfers between devices, sent_together(): lax.all_gather(both, axis, axis=dim, tiled=True)  157 us
    reduce_scatter x3, waiting for transfers between devices, project_down(): lax.psum_scatter(partial_sum.astype(jnp.bfloat16), 'tp', scatter_dimensio...  107 us
    all_gather x3, waiting for transfers between devices, norm_rows(): whole = lax.all_gather(stream, 'tp', axis=1, tiled=True)  63.2 us
    dot_general x3, matrix products, project_down(): jnp.dot(hidden, gathered_copies(weight, 'fs', 1), preferred_element_type=...  27.5 us
    all_to_all x3, starting transfers between devices, copy_for_each(): return lax.all_to_all(copies, axis, split_axis=0, concat_axis=0, tiled=True)  22.3 us
    dot_general x4, matrix products, add_rows(): return jnp.dot(gathered, piece, preferred_element_type=jnp.float32)  15.4 us
  transfers between devices with their start and end apart: 12, of which 9 were waited for; matrix products, arithmetic and copies ran while one was open for 8% of the time, Pallas kernels for 0%

commit v1 on v0

--- a/solution.py
+++ b/solution.py
@@ -32,7 +32,16 @@
 
 
 def norm_rows(stream, gain):
-    whole = lax.all_gather(stream, "tp", axis=1, tiled=True)
+    ways = lax.axis_size("tp")
+    up = [(d, (d + 1) % ways) for d in range(ways)]
+    down = [(d, (d - 1) % ways) for d in range(ways)]
+    earlier, later = ([stream], [stream])
+    for _ in range(ways // 2):
+        earlier.append(lax.ppermute(earlier[-1], "tp", up))
+    for _ in range((ways - 1) // 2):
+        later.append(lax.ppermute(later[-1], "tp", down))
+    line = jnp.concatenate([*earlier[::-1], *later[1:]], axis=1)
+    whole = jnp.roll(line, (lax.axis_index("tp") - ways // 2) * stream.shape[1], axis=1)
     values = whole.astype(jnp.float32)
     scale = lax.rsqrt(jnp.mean(values * values, axis=1, keepdims=True) + epsilon)
     return (values * scale * gain).astype(jnp.bfloat16)

time: 432 us -> 406 us (0.940)
  waiting for transfers between devices: 328 us -> 274 us
  starting transfers between devices: 23 us -> 49.3 us
    ppermute x0 -> x21, waiting for transfers between devices: none -> 71.5 us  [the longest x12 56.1 us: norm_rows(): earlier.append(lax.ppermute(earlier[-1], 'tp', up))]
    all_gather x3, waiting for transfers between devices: 157 us -> 91.8 us  [sent_together(): lax.all_gather(both, axis, axis=dim, tiled=True)]
    all_gather x3 -> x0, waiting for transfers between devices: 63.2 us -> none  [norm_rows(): whole = lax.all_gather(stream, 'tp', axis=1, tiled=True)]
    ppermute x0 -> x21, starting transfers between devices: none -> 26.5 us  [the longest x9 26.4 us: norm_rows(): later.append(lax.ppermute(later[-1], 'tp', down))]
  transfers between devices with their start and end apart: 12 -> 30, of which waited for: 9 -> 20; matrix products, arithmetic and copies ran while one was open for 8% -> 9% of each run, Pallas kernels for 0% -> 0%
where the time goes in v1:
time: 406 us; the launch traced here: 405 us
  waiting for transfers between devices  274 us (67%)
  starting transfers between devices  49.3 us (12%)
  matrix products  43.4 us (11%)
  other arithmetic  16.6 us (4%)
  between operations  13.9 us (3%)
  local copies, waits for them, and re-layouts  7.94 us (2%)
    reduce_scatter x3, waiting for transfers between devices, project_down(): lax.psum_scatter(partial_sum.astype(jnp.bfloat16), 'tp', scatter_dimensio...  110 us
    all_gather x3, waiting for transfers between devices, sent_together(): lax.all_gather(both, axis, axis=dim, tiled=True)  91.8 us
    ppermute x12, waiting for transfers between devices, norm_rows(): earlier.append(lax.ppermute(earlier[-1], 'tp', up))  56.1 us
    dot_general x3, matrix products, project_down(): jnp.dot(hidden, gathered_copies(weight, 'fs', 1), preferred_element_type=...  27.8 us
    ppermute x9, starting transfers between devices, norm_rows(): later.append(lax.ppermute(later[-1], 'tp', down))  26.4 us
    all_to_all x3, starting transfers between devices, copy_for_each(): return lax.all_to_all(copies, axis, split_axis=0, concat_axis=0, tiled=True)  22.1 us
    dot_general x4, matrix products, add_rows(): return jnp.dot(gathered, piece, preferred_element_type=jnp.float32)  15.6 us
    ppermute x9, waiting for transfers between devices, norm_rows(): later.append(lax.ppermute(later[-1], 'tp', down))  15.4 us
  transfers between devices with their start and end apart: 30, of which 20 were waited for; matrix products, arithmetic and copies ran while one was open for 9% of the time, Pallas kernels for 0%

profile of v1, /device:TPU:0, one launch (start us, length us, event | category | flops | bytes accessed | tf_op | source)
XLA Modules:
  0.0 404.8 jit_solution(12831776776340467285)
XLA Ops:
  6.5 1.7 pad_maximum_fusion
  8.3 8.6 %collective-permute-done = bf16[768,256]{1,0:T(8,128)(2,1)S(1)} collective-permute-done((bf16[768,256]{1,0:T(8,128)(2,1)}, bf16[768,256]{1,0:T(8,128)(2,1)S(1)}, u32[]{:S(2)}, u32[]{:S(2)}) %collective-permute-start) | collective-permute-done | bytes 393248 | tf_op jit(solution)/shard_map/ppermute | solution.py:40
  16.9 3.0 collective-permute-start.4
  19.9 5.5 %collective-permute-done.1 = bf16[768,256]{1,0:T(8,128)(2,1)S(1)} collective-permute-done((bf16[768,256]{1,0:T(8,128)(2,1)S(1)}, bf16[768,256]{1,0:T(8,128)(2,1)S(1)}, u32[]{:S(2)}, u32[]{:S(2)}) %collective-permute-start.1) | collective-permute-done | bytes 393248 | tf_op jit(solution)/shard_map/ppermute | solution.py:40
  25.4 0.2 collective-permute-done.4
  25.5 3.4 collective-permute-start.5
  28.9 4.8 %collective-permute-done.2 = bf16[768,256]{1,0:T(8,128)(2,1)S(1)} collective-permute-done((bf16[768,256]{1,0:T(8,128)(2,1)S(1)}, bf16[768,256]{1,0:T(8,128)(2,1)S(1)}, u32[]{:S(2)}, u32[]{:S(2)}) %collective-permute-start.2) | collective-permute-done | bytes 393248 | tf_op jit(solution)/shard_map/ppermute | solution.py:40
  33.8 1.1 copy.16
  34.8 1.8 broadcast_in_dim.6
  36.6 8.2 %all-to-all-start = ((bf16[16,640,128]{1,2,0:T(8,128)(2,1)}), bf16[16,640,128]{1,2,0:T(8,128)(2,1)}, u32[]{:S(2)}, u32[]{:S(2)}) async-start(bf16[16,640,128]{1,2,0:T(8,128)(2,1)} %broadcast_in_dim.6), calls=%async_computation | async-start | bytes 5242880 | tf_op jit(solution)/shard_map/all_to_all | solution.py:20
  44.8 0.0 reduce-scatter.4.cloned.1.call-start
  44.9 2.7 collective-permute-start.6
  48.0 4.9 %collective-permute-done.6 = bf16[768,256]{1,0:T(8,128)(2,1)S(1)} collective-permute-done((bf16[768,256]{1,0:T(8,128)(2,1)S(1)}, bf16[768,256]{1,0:T(8,128)(2,1)S(1)}, u32[]{:S(2)}, u32[]{:S(2)}) %collective-permute-start.6) | collective-permute-done | bytes 393248 | tf_op jit(solution)/shard_map/ppermute | solution.py:42
  52.9 2.3 fusion
  55.2 42.7 %all-gather.4.cloned.1.call-done = bf16[2048,1280]{1,0:T(8,128)(2,1)} async-done(((bf16[128,1280]{1,0:T(8,128)(2,1)}), bf16[2048,1280]{1,0:T(8,128)(2,1)}) %all-gather.4.cloned.1.call-update) | async-done | bytes 5242896 | tf_op jit(solution)/shard_map/all_gather | solution.py:15
  97.9 5.8 %fusion.16 = f32[768,640]{1,0:T(8,128)} fusion(bf16[2048,1280]{1,0:T(8,128)(2,1)} %all-gather.4.cloned.1.call-done, bf16[768,2048]{1,0:T(8,128)(2,1)S(1)} %get-tuple-element.9, f32[2048]{0:T(1024)S(1)} %copy-done.11, f32[768]{0:T(1024)S(1)} %add_rsqrt_fusion.2), kind=kOutput, calls=%fused_computation.31 | convolution fusion | flops 2019557376 | bytes 7744512 | tf_op jit(solution)/shard_map/dot_general | solution.py:51
  103.7 10.7 %convolution_convert_fusion.1 = bf16[768,2048]{1,0:T(8,128)(2,1)} fusion(bf16[640,2048]{0,1:T(8,128)(2,1)} %bitcast.2, f32[768,640]{1,0:T(8,128)} %fusion.16, bf16[2048,1280]{1,0:T(8,128)(2,1)} %all-gather.4.cloned.1.call-done, bf16[768,2048]{1,0:T(8,128)(2,1)S(1)} %get-tuple-element.9, f32[2048]{0:T(1024)S(1)} %copy-done.11, f32[768]{0:T(1024)S(1)} %add_rsqrt_fusion.2), kind=kOutput, calls=%fused_computation.22 | convolution fusion | flops 4037345280 | bytes 13511680 | tf_op jit(solution)/shard_map/dot_general | solution.py:70
  114.5 0.0 all-gather.6.cloned.1.call-start
  114.5 37.2 %reduce-scatter.4.cloned.1.call-done = bf16[768,256]{1,0:T(8,128)(2,1)} async-done(((bf16[768,2048]{1,0:T(8,128)(2,1)}), bf16[768,256]{1,0:T(8,128)(2,1)}) %reduce-scatter.4.cloned.1.call-update) | async-done | bytes 393232 | tf_op jit(solution)/shard_map/reduce_scatter | solution.py:73
  151.8 1.1 add_convert_fusion.2
  152.9 8.4 %collective-permute-done.7 = bf16[768,256]{1,0:T(8,128)(2,1)S(1)} collective-permute-done((bf16[768,256]{1,0:T(8,128)(2,1)S(1)}, bf16[768,256]{1,0:T(8,128)(2,1)S(1)}, u32[]{:S(2)}, u32[]{:S(2)}) %collective-permute-start.7) | collective-permute-done | bytes 393248 | tf_op jit(solution)/shard_map/ppermute | solution.py:40
  161.3 0.7 pad_maximum_fusion.2
  162.0 3.0 collective-permute-start.11
  165.0 4.8 %collective-permute-done.8 = bf16[768,256]{1,0:T(8,128)(2,1)S(1)} collective-permute-done((bf16[768,256]{1,0:T(8,128)(2,1)S(1)}, bf16[768,256]{1,0:T(8,128)(2,1)S(1)}, u32[]{:S(2)}, u32[]{:S(2)}) %collective-permute-start.8) | collective-permute-done | bytes 393248 | tf_op jit(solution)/shard_map/ppermute | solution.py:40
  169.7 0.5 collective-permute-done.11
  170.3 3.1 collective-permute-start.12
  173.4 4.8 %collective-permute-done.9 = bf16[768,256]{1,0:T(8,128)(2,1)S(1)} collective-permute-done((bf16[768,256]{1,0:T(8,128)(2,1)S(1)}, bf16[768,256]{1,0:T(8,128)(2,1)S(1)}, u32[]{:S(2)}, u32[]{:S(2)}) %collective-permute-start.9) | collective-permute-done | bytes 393248 | tf_op jit(solution)/shard_map/ppermute | solution.py:40
  178.1 0.1 copy.17
  178.3 0.9 broadcast_in_dim.7
  179.2 7.0 %all-to-all-start.1 = ((bf16[16,128,128]{1,2,0:T(8,128)(2,1)}), bf16[16,128,128]{1,2,0:T(8,128)(2,1)}, u32[]{:S(2)}, u32[]{:S(2)}) async-start(bf16[16,128,128]{1,2,0:T(8,128)(2,1)} %broadcast_in_dim.7), calls=%async_computation.2 | async-start | bytes 1048576 | tf_op jit(solution)/shard_map/all_to_all | solution.py:20
  186.2 0.2 reduce-scatter.6.cloned.1.call-start
  186.4 2.7 collective-permute-start.13
  189.2 0.1 constant_dynamic-update-slice_fusion.14
  189.5 4.9 %collective-permute-done.13 = bf16[768,256]{1,0:T(8,128)(2,1)S(1)} collective-permute-done((bf16[768,256]{1,0:T(8,128)(2,1)S(1)}, bf16[768,256]{1,0:T(8,128)(2,1)S(1)}, u32[]{:S(2)}, u32[]{:S(2)}) %collective-permute-start.13) | collective-permute-done | bytes 393248 | tf_op jit(solution)/shard_map/ppermute | solution.py:42
  194.5 1.8 fusion.3
  196.2 2.2 fusion.5
  198.5 11.9 %all-gather.6.cloned.1.call-done = bf16[2048,384]{1,0:T(8,128)(2,1)} async-done(((bf16[128,384]{1,0:T(8,128)(2,1)}), bf16[2048,384]{1,0:T(8,128)(2,1)}) %all-gather.6.cloned.1.call-update) | async-done | bytes 1572880 | tf_op jit(solution)/shard_map/all_gather | solution.py:15
  210.3 2.0 fusion.43
  212.4 2.0 convolution_multiply_fusion
  214.4 0.9 fusion.50
  215.3 6.4 %convolution_convert_fusion.2 = bf16[768,2048]{1,0:T(8,128)(2,1)} fusion(bf16[128,2048]{0,1:T(8,128)(2,1)} %bitcast.9, f32[768,128]{1,0:T(8,128)} %bitcast.30, bf16[768,2048]{1,0:T(8,128)(2,1)S(1)} %fusion.5, bf16[2048,384]{1,0:T(8,128)(2,1)} %all-gather.6.cloned.1.call-done), kind=kOutput, calls=%fused_computation.23 | convolution fusion | flops 807075840 | bytes 7733248 | tf_op jit(solution)/shard_map/dot_general | solution.py:70
  221.7 0.0 all-gather.8.cloned.1.call-start
  221.7 0.8 copy-done.2
  222.5 0.1 copy-done.3
  222.6 0.7 pad_maximum_fusion.1
  223.4 33.6 %reduce-scatter.6.cloned.1.call-done = bf16[768,256]{1,0:T(8,128)(2,1)} async-done(((bf16[768,2048]{1,0:T(8,128)(2,1)}), bf16[768,256]{1,0:T(8,128)(2,1)}) %reduce-scatter.6.cloned.1.call-update) | async-done | bytes 393232 | tf_op jit(solution)/shard_map/reduce_scatter | solution.py:73
  257.0 1.1 add_convert_fusion.1
  258.1 8.4 %collective-permute-done.14 = bf16[768,256]{1,0:T(8,128)(2,1)S(1)} collective-permute-done((bf16[768,256]{1,0:T(8,128)(2,1)S(1)}, bf16[768,256]{1,0:T(8,128)(2,1)S(1)}, u32[]{:S(2)}, u32[]{:S(2)}) %collective-permute-start.14) | collective-permute-done | bytes 393248 | tf_op jit(solution)/shard_map/ppermute | solution.py:40
  266.5 3.0 collective-permute-start.18
  269.5 5.5 %collective-permute-done.15 = bf16[768,256]{1,0:T(8,128)(2,1)S(1)} collective-permute-done((bf16[768,256]{1,0:T(8,128)(2,1)S(1)}, bf16[768,256]{1,0:T(8,128)(2,1)S(1)}, u32[]{:S(2)}, u32[]{:S(2)}) %collective-permute-start.15) | collective-permute-done | bytes 393248 | tf_op jit(solution)/shard_map/ppermute | solution.py:40
  274.9 3.0 collective-permute-start.19
  277.9 5.4 %collective-permute-done.16 = bf16[768,256]{1,0:T(8,128)(2,1)S(1)} collective-permute-done((bf16[768,256]{1,0:T(8,128)(2,1)S(1)}, bf16[768,256]{1,0:T(8,128)(2,1)S(1)}, u32[]{:S(2)}, u32[]{:S(2)}) %collective-permute-start.16) | collective-permute-done | bytes 393248 | tf_op jit(solution)/shard_map/ppermute | solution.py:40
  283.3 0.2 copy.18
  283.5 1.8 broadcast_in_dim.8
  285.3 7.0 %all-to-all-start.2 = ((bf16[16,640,128]{1,2,0:T(8,128)(2,1)}), bf16[16,640,128]{1,2,0:T(8,128)(2,1)}, u32[]{:S(2)}, u32[]{:S(2)}) async-start(bf16[16,640,128]{1,2,0:T(8,128)(2,1)} %broadcast_in_dim.8), calls=%async_computation.4 | async-start | bytes 5242880 | tf_op jit(solution)/shard_map/all_to_all | solution.py:20
  292.3 0.3 reduce-scatter.8.cloned.1.call-start
  292.6 2.7 collective-permute-start.20
  295.6 4.9 %collective-permute-done.20 = bf16[768,256]{1,0:T(8,128)(2,1)S(1)} collective-permute-done((bf16[768,256]{1,0:T(8,128)(2,1)S(1)}, bf16[768,256]{1,0:T(8,128)(2,1)S(1)}, u32[]{:S(2)}, u32[]{:S(2)}) %collective-permute-start.20) | collective-permute-done | bytes 393248 | tf_op jit(solution)/shard_map/ppermute | solution.py:42
  300.6 2.3 fusion.6
  302.9 37.2 %all-gather.8.cloned.1.call-done = bf16[2048,1280]{1,0:T(8,128)(2,1)} async-done(((bf16[128,1280]{1,0:T(8,128)(2,1)}), bf16[2048,1280]{1,0:T(8,128)(2,1)}) %all-gather.8.cloned.1.call-update) | async-done | bytes 5242896 | tf_op jit(solution)/shard_map/all_gather | solution.py:15
  340.1 5.8 %fusion.12 = f32[768,640]{1,0:T(8,128)} fusion(bf16[2048,1280]{1,0:T(8,128)(2,1)} %all-gather.8.cloned.1.call-done, bf16[768,2048]{1,0:T(8,128)(2,1)S(1)} %get-tuple-element.7, f32[2048]{0:T(1024)S(1)} %copy-done.12, f32[768]{0:T(1024)S(1)} %add_rsqrt_fusion), kind=kOutput, calls=%fused_computation.27 | convolution fusion | flops 2019557376 | bytes 7744512 | tf_op jit(solution)/shard_map/dot_general | solution.py:51
  345.9 10.7 %convolution_convert_fusion = bf16[768,2048]{1,0:T(8,128)(2,1)} fusion(bf16[640,2048]{0,1:T(8,128)(2,1)} %bitcast.11, f32[768,640]{1,0:T(8,128)} %fusion.12, bf16[2048,1280]{1,0:T(8,128)(2,1)} %all-gather.8.cloned.1.call-done, bf16[768,2048]{1,0:T(8,128)(2,1)S(1)} %get-tuple-element.7, f32[2048]{0:T(1024)S(1)} %copy-done.12, f32[768]{0:T(1024)S(1)} %add_rsqrt_fusion), kind=kOutput, calls=%fused_computation.21 | convolution fusion | flops 4037345280 | bytes 13511680 | tf_op jit(solution)/shard_map/dot_general | solution.py:70
  356.6 39.5 %reduce-scatter.8.cloned.1.call-done = bf16[768,256]{1,0:T(8,128)(2,1)} async-done(((bf16[768,2048]{1,0:T(8,128)(2,1)}), bf16[768,256]{1,0:T(8,128)(2,1)}) %reduce-scatter.8.cloned.1.call-update) | async-done | bytes 393232 | tf_op jit(solution)/shard_map/reduce_scatter | solution.py:73
  396.1 1.9 add_convert_fusion
  (80 shorter events, 1.3 us)
Async XLA Ops:
  6.5 91.4 %all-gather.4.cloned.1.call-start = ((), (), s32[]{:S(2)}) async-start(), calls=%async_computation.6 | async-start | bytes 5570560 | tf_op jit(solution)/shard_map/all_gather | solution.py:15
  8.3 8.6 %collective-permute-start = (bf16[768,256]{1,0:T(8,128)(2,1)}, bf16[768,256]{1,0:T(8,128)(2,1)S(1)}, u32[]{:S(2)}, u32[]{:S(2)}) collective-permute-start(bf16[768,256]{1,0:T(8,128)(2,1)} %bitcast.27), channel_id=1, source_target_pairs={{0,1},{1,2},{2,3},{3,4},{4,5},{5,6},{6,7},{7,0},{8,9},{9,10},{10,1... | collective-permute-start | bytes 1179656 | tf_op jit(solution)/shard_map/ppermute | solution.py:40
  16.9 8.4 %collective-permute-start.1 = (bf16[768,256]{1,0:T(8,128)(2,1)S(1)}, bf16[768,256]{1,0:T(8,128)(2,1)S(1)}, u32[]{:S(2)}, u32[]{:S(2)}) collective-permute-start(bf16[768,256]{1,0:T(8,128)(2,1)S(1)} %collective-permute-done), channel_id=1, source_target_pairs={{0,1},{1,2},{2,3},{3,4},{4,5},{5,6},{6,7},{7,0},{8,9},{9,10},{10,1... | collective-permute-start | bytes 1179656 | tf_op jit(solution)/shard_map/ppermute | solution.py:40
  16.9 8.6 %collective-permute-start.4 = (bf16[768,256]{1,0:T(8,128)(2,1)}, bf16[768,256]{1,0:T(8,128)(2,1)S(1)}, u32[]{:S(2)}, u32[]{:S(2)}) collective-permute-start(bf16[768,256]{1,0:T(8,128)(2,1)} %bitcast.28), channel_id=1, source_target_pairs={{0,7},{1,0},{2,1},{3,2},{4,3},{5,4},{6,5},{7,6},{8,15},{9,8},{10,9... | collective-permute-start | bytes 1179656 | tf_op jit(solution)/shard_map/ppermute | solution.py:42
  25.4 8.4 %collective-permute-start.2 = (bf16[768,256]{1,0:T(8,128)(2,1)S(1)}, bf16[768,256]{1,0:T(8,128)(2,1)S(1)}, u32[]{:S(2)}, u32[]{:S(2)}) collective-permute-start(bf16[768,256]{1,0:T(8,128)(2,1)S(1)} %collective-permute-done.1), channel_id=1, source_target_pairs={{0,1},{1,2},{2,3},{3,4},{4,5},{5,6},{6,7},{7,0},{8,9},{9,10},{10,1... | collective-permute-start | bytes 1179656 | tf_op jit(solution)/shard_map/ppermute | solution.py:40
  25.5 19.4 %collective-permute-start.5 = (bf16[768,256]{1,0:T(8,128)(2,1)S(1)}, bf16[768,256]{1,0:T(8,128)(2,1)S(1)}, u32[]{:S(2)}, u32[]{:S(2)}) collective-permute-start(bf16[768,256]{1,0:T(8,128)(2,1)S(1)} %collective-permute-done.4), channel_id=1, source_target_pairs={{0,7},{1,0},{2,1},{3,2},{4,3},{5,4},{6,5},{7,6},{8,15},{9,8},{10,9... | collective-permute-start | bytes 1179656 | tf_op jit(solution)/shard_map/ppermute | solution.py:42
  33.8 13.8 %collective-permute-start.3 = (bf16[768,256]{1,0:T(8,128)(2,1)S(1)}, bf16[768,256]{1,0:T(8,128)(2,1)S(1)}, u32[]{:S(2)}, u32[]{:S(2)}) collective-permute-start(bf16[768,256]{1,0:T(8,128)(2,1)S(1)} %collective-permute-done.2), channel_id=1, source_target_pairs={{0,1},{1,2},{2,3},{3,4},{4,5},{5,6},{6,7},{7,0},{8,9},{9,10},{10,1... | collective-permute-start | bytes 1179656 | tf_op jit(solution)/shard_map/ppermute | solution.py:40
  36.6 11.2 %copy-start = (bf16[2,384,256]{2,1,0:T(8,128)(2,1)S(1)}, bf16[2,384,256]{2,1,0:T(8,128)(2,1)}, u32[]{:S(2)}) copy-start(bf16[2,384,256]{2,1,0:T(8,128)(2,1)} %param.17) | copy-start | bytes 1179652
  36.6 67.1 %all-to-all-start = ((bf16[16,640,128]{1,2,0:T(8,128)(2,1)}), bf16[16,640,128]{1,2,0:T(8,128)(2,1)}, u32[]{:S(2)}, u32[]{:S(2)}) async-start(bf16[16,640,128]{1,2,0:T(8,128)(2,1)} %broadcast_in_dim.6), calls=%async_computation | async-start | bytes 5242880 | tf_op jit(solution)/shard_map/all_to_all | solution.py:20
  44.8 106.9 %reduce-scatter.4.cloned.1.call-start = ((), (), s32[]{:S(2)}) async-start(), calls=%async_computation.7 | async-start | bytes 3538944 | tf_op jit(solution)/shard_map/reduce_scatter | solution.py:73
  44.9 8.0 %collective-permute-start.6 = (bf16[768,256]{1,0:T(8,128)(2,1)S(1)}, bf16[768,256]{1,0:T(8,128)(2,1)S(1)}, u32[]{:S(2)}, u32[]{:S(2)}) collective-permute-start(bf16[768,256]{1,0:T(8,128)(2,1)S(1)} %collective-permute-done.5), channel_id=1, source_target_pairs={{0,7},{1,0},{2,1},{3,2},{4,3},{5,4},{6,5},{7,6},{8,15},{9,8},{10,9... | collective-permute-start | bytes 1179656 | tf_op jit(solution)/shard_map/ppermute | solution.py:42
  52.9 45.0 %copy-start.11 = (f32[2048]{0:T(1024)S(1)}, f32[2048]{0:T(1024)}, u32[]{:S(2)}) copy-start(f32[2048]{0:T(1024)} %param.18) | copy-start | bytes 24580
  114.4 37.3 %copy-start.1 = (bf16[2,384,256]{2,1,0:T(8,128)(2,1)S(1)}, bf16[2,384,256]{2,1,0:T(8,128)(2,1)}, u32[]{:S(2)}) copy-start(bf16[2,384,256]{2,1,0:T(8,128)(2,1)} %param.17) | copy-start | bytes 1179652
  114.4 46.9 %copy-start.6 = (bf16[128,128]{1,0:T(8,128)(2,1)S(1)}, bf16[128,128]{1,0:T(8,128)(2,1)}, u32[]{:S(2)}) copy-start(bf16[128,128]{1,0:T(8,128)(2,1)} %param.25) | copy-start | bytes 98308
  114.4 46.9 %copy-start.7 = (bf16[128,128]{1,0:T(8,128)(2,1)S(1)}, bf16[128,128]{1,0:T(8,128)(2,1)}, u32[]{:S(2)}) copy-start(bf16[128,128]{1,0:T(8,128)(2,1)} %param.24) | copy-start | bytes 98308
  114.4 46.9 %copy-start.8 = (bf16[128,128]{1,0:T(8,128)(2,1)S(1)}, bf16[128,128]{1,0:T(8,128)(2,1)}, u32[]{:S(2)}) copy-start(bf16[128,128]{1,0:T(8,128)(2,1)} %param.23) | copy-start | bytes 98308
  114.4 63.7 %copy-start.5 = (bf16[128,128]{1,0:T(8,128)(2,1)S(1)}, bf16[128,128]{1,0:T(8,128)(2,1)}, u32[]{:S(2)}) copy-start(bf16[128,128]{1,0:T(8,128)(2,1)} %param.27) | copy-start | bytes 98308
  114.4 72.0 %copy-start.10 = (f32[3,128]{1,0:T(4,128)S(1)}, f32[3,128]{1,0:T(4,128)}, u32[]{:S(2)}) copy-start(f32[3,128]{1,0:T(4,128)} %param.26) | copy-start | bytes 4612
  114.5 95.8 %all-gather.6.cloned.1.call-start = ((), (), s32[]{:S(2)}) async-start(), calls=%async_computation.8 | async-start | bytes 1671168 | tf_op jit(solution)/shard_map/all_gather | solution.py:15
  152.9 8.4 %collective-permute-start.7 = (bf16[768,256]{1,0:T(8,128)(2,1)S(1)}, bf16[768,256]{1,0:T(8,128)(2,1)S(1)}, u32[]{:S(2)}, u32[]{:S(2)}) collective-permute-start(bf16[768,256]{1,0:T(8,128)(2,1)S(1)} %add_convert_fusion.2), channel_id=1, source_target_pairs={{0,1},{1,2},{2,3},{3,4},{4,5},{5,6},{6,7},{7,0},{8,9},{9,10},{10,1... | collective-permute-start | bytes 1179656 | tf_op jit(solution)/shard_map/ppermute | solution.py:40
  161.3 8.4 %collective-permute-start.8 = (bf16[768,256]{1,0:T(8,128)(2,1)S(1)}, bf16[768,256]{1,0:T(8,128)(2,1)S(1)}, u32[]{:S(2)}, u32[]{:S(2)}) collective-permute-start(bf16[768,256]{1,0:T(8,128)(2,1)S(1)} %collective-permute-done.7), channel_id=1, source_target_pairs={{0,1},{1,2},{2,3},{3,4},{4,5},{5,6},{6,7},{7,0},{8,9},{9,10},{10,1... | collective-permute-start | bytes 1179656 | tf_op jit(solution)/shard_map/ppermute | solution.py:40
  162.0 8.3 %collective-permute-start.11 = (bf16[768,256]{1,0:T(8,128)(2,1)S(1)}, bf16[768,256]{1,0:T(8,128)(2,1)S(1)}, u32[]{:S(2)}, u32[]{:S(2)}) collective-permute-start(bf16[768,256]{1,0:T(8,128)(2,1)S(1)} %add_convert_fusion.2), channel_id=1, source_target_pairs={{0,7},{1,0},{2,1},{3,2},{4,3},{5,4},{6,5},{7,6},{8,15},{9,8},{10,9... | collective-permute-start | bytes 1179656 | tf_op jit(solution)/shard_map/ppermute | solution.py:42
  169.7 8.4 %collective-permute-start.9 = (bf16[768,256]{1,0:T(8,128)(2,1)S(1)}, bf16[768,256]{1,0:T(8,128)(2,1)S(1)}, u32[]{:S(2)}, u32[]{:S(2)}) collective-permute-start(bf16[768,256]{1,0:T(8,128)(2,1)S(1)} %collective-permute-done.8), channel_id=1, source_target_pairs={{0,1},{1,2},{2,3},{3,4},{4,5},{5,6},{6,7},{7,0},{8,9},{9,10},{10,1... | collective-permute-start | bytes 1179656 | tf_op jit(solution)/shard_map/ppermute | solution.py:40
  170.3 16.2 %collective-permute-start.12 = (bf16[768,256]{1,0:T(8,128)(2,1)S(1)}, bf16[768,256]{1,0:T(8,128)(2,1)S(1)}, u32[]{:S(2)}, u32[]{:S(2)}) collective-permute-start(bf16[768,256]{1,0:T(8,128)(2,1)S(1)} %collective-permute-done.11), channel_id=1, source_target_pairs={{0,7},{1,0},{2,1},{3,2},{4,3},{5,4},{6,5},{7,6},{8,15},{9,8},{10,9... | collective-permute-start | bytes 1179656 | tf_op jit(solution)/shard_map/ppermute | solution.py:42
  178.1 11.0 %collective-permute-start.10 = (bf16[768,256]{1,0:T(8,128)(2,1)S(1)}, bf16[768,256]{1,0:T(8,128)(2,1)S(1)}, u32[]{:S(2)}, u32[]{:S(2)}) collective-permute-start(bf16[768,256]{1,0:T(8,128)(2,1)S(1)} %collective-permute-done.9), channel_id=1, source_target_pairs={{0,1},{1,2},{2,3},{3,4},{4,5},{5,6},{6,7},{7,0},{8,9},{9,10},{10,1... | collective-permute-start | bytes 1179656 | tf_op jit(solution)/shard_map/ppermute | solution.py:40
  179.2 36.1 %all-to-all-start.1 = ((bf16[16,128,128]{1,2,0:T(8,128)(2,1)}), bf16[16,128,128]{1,2,0:T(8,128)(2,1)}, u32[]{:S(2)}, u32[]{:S(2)}) async-start(bf16[16,128,128]{1,2,0:T(8,128)(2,1)} %broadcast_in_dim.7), calls=%async_computation.2 | async-start | bytes 1048576 | tf_op jit(solution)/shard_map/all_to_all | solution.py:20
  186.2 70.8 %reduce-scatter.6.cloned.1.call-start = ((), (), s32[]{:S(2)}) async-start(), calls=%async_computation.9 | async-start | bytes 3538944 | tf_op jit(solution)/shard_map/reduce_scatter | solution.py:73
  186.4 8.0 %collective-permute-start.13 = (bf16[768,256]{1,0:T(8,128)(2,1)S(1)}, bf16[768,256]{1,0:T(8,128)(2,1)S(1)}, u32[]{:S(2)}, u32[]{:S(2)}) collective-permute-start(bf16[768,256]{1,0:T(8,128)(2,1)S(1)} %collective-permute-done.12), channel_id=1, source_target_pairs={{0,7},{1,0},{2,1},{3,2},{4,3},{5,4},{6,5},{7,6},{8,15},{9,8},{10,9... | collective-permute-start | bytes 1179656 | tf_op jit(solution)/shard_map/ppermute | solution.py:42
  189.3 6.9 %copy-start.9 = (f32[2048]{0:T(1024)S(1)}, f32[2048]{0:T(1024)}, u32[]{:S(2)}) copy-start(f32[2048]{0:T(1024)} %param.22) | copy-start | bytes 24580
  221.6 0.9 copy-start.2
  221.6 1.0 copy-start.3
  221.6 61.7 %copy-start.4 = (bf16[640,128]{1,0:T(8,128)(2,1)S(1)}, bf16[640,128]{1,0:T(8,128)(2,1)}, u32[]{:S(2)}) copy-start(bf16[640,128]{1,0:T(8,128)(2,1)} %param.31) | copy-start | bytes 491524
  221.7 118.5 %all-gather.8.cloned.1.call-start = ((), (), s32[]{:S(2)}) async-start(), calls=%async_computation.10 | async-start | bytes 5570560 | tf_op jit(solution)/shard_map/all_gather | solution.py:15
  258.1 8.4 %collective-permute-start.14 = (bf16[768,256]{1,0:T(8,128)(2,1)S(1)}, bf16[768,256]{1,0:T(8,128)(2,1)S(1)}, u32[]{:S(2)}, u32[]{:S(2)}) collective-permute-start(bf16[768,256]{1,0:T(8,128)(2,1)S(1)} %add_convert_fusion.1), channel_id=1, source_target_pairs={{0,1},{1,2},{2,3},{3,4},{4,5},{5,6},{6,7},{7,0},{8,9},{9,10},{10,1... | collective-permute-start | bytes 1179656 | tf_op jit(solution)/shard_map/ppermute | solution.py:40
  266.5 8.4 %collective-permute-start.15 = (bf16[768,256]{1,0:T(8,128)(2,1)S(1)}, bf16[768,256]{1,0:T(8,128)(2,1)S(1)}, u32[]{:S(2)}, u32[]{:S(2)}) collective-permute-start(bf16[768,256]{1,0:T(8,128)(2,1)S(1)} %collective-permute-done.14), channel_id=1, source_target_pairs={{0,1},{1,2},{2,3},{3,4},{4,5},{5,6},{6,7},{7,0},{8,9},{9,10},{10,1... | collective-permute-start | bytes 1179656 | tf_op jit(solution)/shard_map/ppermute | solution.py:40
  266.5 8.4 %collective-permute-start.18 = (bf16[768,256]{1,0:T(8,128)(2,1)S(1)}, bf16[768,256]{1,0:T(8,128)(2,1)S(1)}, u32[]{:S(2)}, u32[]{:S(2)}) collective-permute-start(bf16[768,256]{1,0:T(8,128)(2,1)S(1)} %add_convert_fusion.1), channel_id=1, source_target_pairs={{0,7},{1,0},{2,1},{3,2},{4,3},{5,4},{6,5},{7,6},{8,15},{9,8},{10,9... | collective-permute-start | bytes 1179656 | tf_op jit(solution)/shard_map/ppermute | solution.py:42
  274.9 8.4 %collective-permute-start.16 = (bf16[768,256]{1,0:T(8,128)(2,1)S(1)}, bf16[768,256]{1,0:T(8,128)(2,1)S(1)}, u32[]{:S(2)}, u32[]{:S(2)}) collective-permute-start(bf16[768,256]{1,0:T(8,128)(2,1)S(1)} %collective-permute-done.15), channel_id=1, source_target_pairs={{0,1},{1,2},{2,3},{3,4},{4,5},{5,6},{6,7},{7,0},{8,9},{9,10},{10,1... | collective-permute-start | bytes 1179656 | tf_op jit(solution)/shard_map/ppermute | solution.py:40
  274.9 17.6 %collective-permute-start.19 = (bf16[768,256]{1,0:T(8,128)(2,1)S(1)}, bf16[768,256]{1,0:T(8,128)(2,1)S(1)}, u32[]{:S(2)}, u32[]{:S(2)}) collective-permute-start(bf16[768,256]{1,0:T(8,128)(2,1)S(1)} %collective-permute-done.18), channel_id=1, source_target_pairs={{0,7},{1,0},{2,1},{3,2},{4,3},{5,4},{6,5},{7,6},{8,15},{9,8},{10,9... | collective-permute-start | bytes 1179656 | tf_op jit(solution)/shard_map/ppermute | solution.py:42
  283.3 11.9 %collective-permute-start.17 = (bf16[768,256]{1,0:T(8,128)(2,1)S(1)}, bf16[768,256]{1,0:T(8,128)(2,1)S(1)}, u32[]{:S(2)}, u32[]{:S(2)}) collective-permute-start(bf16[768,256]{1,0:T(8,128)(2,1)S(1)} %collective-permute-done.16), channel_id=1, source_target_pairs={{0,1},{1,2},{2,3},{3,4},{4,5},{5,6},{6,7},{7,0},{8,9},{9,10},{10,1... | collective-permute-start | bytes 1179656 | tf_op jit(solution)/shard_map/ppermute | solution.py:40
  285.3 60.6 %all-to-all-start.2 = ((bf16[16,640,128]{1,2,0:T(8,128)(2,1)}), bf16[16,640,128]{1,2,0:T(8,128)(2,1)}, u32[]{:S(2)}, u32[]{:S(2)}) async-start(bf16[16,640,128]{1,2,0:T(8,128)(2,1)} %broadcast_in_dim.8), calls=%async_computation.4 | async-start | bytes 5242880 | tf_op jit(solution)/shard_map/all_to_all | solution.py:20
  292.3 103.8 %reduce-scatter.8.cloned.1.call-start = ((), (), s32[]{:S(2)}) async-start(), calls=%async_computation.11 | async-start | bytes 3538944 | tf_op jit(solution)/shard_map/reduce_scatter | solution.py:73
  292.6 8.0 %collective-permute-start.20 = (bf16[768,256]{1,0:T(8,128)(2,1)S(1)}, bf16[768,256]{1,0:T(8,128)(2,1)S(1)}, u32[]{:S(2)}, u32[]{:S(2)}) collective-permute-start(bf16[768,256]{1,0:T(8,128)(2,1)S(1)} %collective-permute-done.19), channel_id=1, source_target_pairs={{0,7},{1,0},{2,1},{3,2},{4,3},{5,4},{6,5},{7,6},{8,15},{9,8},{10,9... | collective-permute-start | bytes 1179656 | tf_op jit(solution)/shard_map/ppermute | solution.py:42
  300.6 39.5 %copy-start.12 = (f32[2048]{0:T(1024)S(1)}, f32[2048]{0:T(1024)}, u32[]{:S(2)}) copy-start(f32[2048]{0:T(1024)} %param.28) | copy-start | bytes 24580
Sparse Core Ops, SparseCore 0:
  9.5 88.4 all-gather.3
  114.6 37.1 reduce-scatter.3
  162.1 48.1 all-gather.5
  221.8 35.1 reduce-scatter.5
  259.0 81.1 all-gather.7
  356.8 39.3 reduce-scatter.7
